TPU v7x, 32 devices: a whole 2x2x4 slice. The times are simulated.
32 devices in a mesh: sp: 8 (over z, core), tp: 4 (over y, x).
Axes of the slice: x: 2, y: 2, z: 4, core: 2. Of those that a mesh axis runs over, the one named last changes fastest.
Arguments:
- residual: bfloat16 [2048, 2048], P('sp'), may hold values from -6 to 6
- queries: bfloat16 [2048, 16, 128], P('sp', 'tp'), may hold values from -256 to 256
- key_vectors: bfloat16 [2048, 16, 128], P('sp', 'tp'), may hold values from -5.3 to 5.3
- value_rows: bfloat16 [2048, 16, 128], P('sp', 'tp'), may hold values from -6 to 6
- head_lambda: float32 [16], P('tp'), may hold values from 0.3 to 0.8
- head_gain: float32 [128], replicated, may hold values from 0.1 to 1.9
- out_weight: bfloat16 [2048, 2048], P('tp'), may hold values from -0.125 to 0.125
- ffn_gain: float32 [2048], replicated, may hold values from 0.1 to 1.9
- expert_gate: bfloat16 [8, 2048, 4096], P('sp', None, 'tp'), may hold values from -0.125 to 0.125
- expert_up: bfloat16 [8, 2048, 4096], P('sp', None, 'tp'), may hold values from -0.125 to 0.125
- expert_down: bfloat16 [8, 4096, 2048], P('sp', None, 'tp'), may hold values from -0.09375 to 0.09375
- routing: int32 [2048, 2], P('sp'), may hold values from 0 to 7, as said below
- route_weight: float32 [2048, 2], P('sp'), may hold values from 0.1 to 0.9
Outputs:
- layer_out: bfloat16 [2048, 2048], P('sp')
Inputs may be any that keep to these rules, and one draw needn't show every extreme that they name: `routing`: each row names two different experts of one group of 2 consecutive experts. In each aligned block of 256 rows no expert is named by more than 128 rows, and in every block some expert is named by exactly 128 rows.
All inputs are finite; a program needn't handle non-finite values.
Results may differ from a plain program's by a relative error of at most 0.015.
Values may be sent and summed in bfloat16 or wider, within the bound.
A program may use at most 64 MiB of HBM per device.

v0:
```python
import math

import jax
import jax.numpy as jnp
from jax import lax
from jax.sharding import PartitionSpec as P

GROUPS = 4


norm_eps = 1e-06


def online_update(running, query_part, key_part, value_part, query_pos, key_pos, score_scale):
    highest, totals, accum = running
    scores = (
        jnp.einsum("qhd,khd->hqk", query_part, key_part, preferred_element_type=jnp.float32)
        * score_scale
    )
    scores = jnp.where(key_pos[None, None, :] <= query_pos[None, :, None], scores, -jnp.inf)
    new_high = jnp.maximum(highest, jnp.max(scores, axis=-1))
    shrink = jnp.exp(highest - new_high)
    weights = jnp.exp(scores - new_high[:, :, None])
    totals = shrink * totals + jnp.sum(weights, axis=-1)
    blended = jnp.einsum(
        "hqk,khe->qhe", weights.astype(jnp.bfloat16), value_part, preferred_element_type=jnp.float32
    )
    accum = jnp.transpose(shrink)[:, :, None] * accum + blended
    return (new_high, totals, accum)


def shards(
    residual,
    queries,
    key_vectors,
    value_rows,
    head_lambda,
    head_gain,
    out_weight,
    ffn_gain,
    expert_gate,
    expert_up,
    expert_down,
    routing,
    route_weight,
):
    tok_count = queries.shape[0]
    local_heads = queries.shape[1]
    half_width = queries.shape[2] // 2
    value_width = value_rows.shape[2]
    score_scale = half_width ** (-0.5)
    query_pos = lax.axis_index("sp") * tok_count + jnp.arange(tok_count, dtype=jnp.int32)
    last_query = query_pos[-1]
    first_half = queries[:, :, :half_width]
    second_half = queries[:, :, half_width:]
    start_high = jnp.full((local_heads, tok_count), -1e30, jnp.float32)
    start_total = jnp.zeros((local_heads, tok_count), jnp.float32)
    start_accum = jnp.zeros((tok_count, local_heads, value_width), jnp.float32)
    empty_state = (start_high, start_total, start_accum)
    running = (empty_state, empty_state)
    key_piece = lax.all_gather(key_vectors, "sp", axis=0, tiled=True)
    value_piece = lax.all_gather(value_rows, "sp", axis=0, tiled=True)
    piece_len = key_piece.shape[0]
    block_len = math.gcd(piece_len, 512)
    block_count = piece_len // block_len
    key_blocks = key_piece.reshape(block_count, block_len, local_heads, 2 * half_width)
    value_blocks = value_piece.reshape(block_count, block_len, local_heads, value_width)

    def visit(current, stacked):
        block_index, key_block, value_block = stacked
        block_first = block_index * block_len
        key_pos = block_first + jnp.arange(block_len, dtype=jnp.int32)

        def compute(inside):
            first_state = online_update(
                inside[0],
                first_half,
                key_block[:, :, :half_width],
                value_block,
                query_pos,
                key_pos,
                score_scale,
            )
            second_state = online_update(
                inside[1],
                second_half,
                key_block[:, :, half_width:],
                value_block,
                query_pos,
                key_pos,
                score_scale,
            )
            return (first_state, second_state)

        return (lax.cond(block_first <= last_query, compute, lambda inside: inside, current), None)

    running, _ = lax.scan(
        visit, running, (jnp.arange(block_count, dtype=jnp.int32), key_blocks, value_blocks)
    )
    first_state, second_state = running
    first_out = first_state[2] / jnp.transpose(first_state[1])[:, :, None]
    second_out = second_state[2] / jnp.transpose(second_state[1])[:, :, None]
    combined = first_out - head_lambda[None, :, None] * second_out
    normed_heads = (
        combined
        * lax.rsqrt(jnp.mean(combined * combined, axis=-1, keepdims=True) + norm_eps)
        * head_gain
    )
    attended = normed_heads.astype(jnp.bfloat16).reshape(tok_count, local_heads * value_width)
    partial_proj = jnp.dot(attended, out_weight, preferred_element_type=jnp.float32)
    projected = lax.psum(partial_proj.astype(jnp.bfloat16), "tp").astype(jnp.float32)
    stream = residual.astype(jnp.float32) + projected
    block_normed = (
        stream * lax.rsqrt(jnp.mean(stream * stream, axis=-1, keepdims=True) + norm_eps) * ffn_gain
    ).astype(jnp.bfloat16)
    expert_count = lax.axis_size("sp")
    tp_count = lax.axis_size("tp")
    per_group = expert_count // GROUPS
    capacity = tok_count // per_group
    top_count = routing.shape[1]
    model_width = block_normed.shape[1]
    flat_routes = routing.reshape(-1)
    route_count = flat_routes.shape[0]
    onehot = (flat_routes[:, None] == jnp.arange(expert_count, dtype=jnp.int32)[None, :]).astype(
        jnp.int32
    )
    earlier = jnp.cumsum(onehot, axis=0) - onehot
    position = jnp.sum(earlier * onehot, axis=1)
    slot_index = flat_routes * capacity + position
    slot_token = (
        jnp.full((expert_count * capacity,), tok_count, jnp.int32)
        .at[slot_index]
        .set(jnp.arange(route_count, dtype=jnp.int32) // top_count)
    )
    slot_table = slot_token.reshape(expert_count, capacity)
    slice_width = model_width // tp_count
    own_columns = lax.dynamic_slice_in_dim(
        block_normed, lax.axis_index("tp") * slice_width, slice_width, 1
    )
    outgoing = jnp.take(own_columns, slot_table, axis=0, mode="fill", fill_value=0)
    landed = lax.all_to_all(outgoing, "sp", split_axis=0, concat_axis=0, tiled=True)
    arrived = lax.all_gather(landed, "tp", axis=2, tiled=True)
    expert_rows = arrived.reshape(-1, model_width)
    gate_part = jnp.dot(expert_rows, expert_gate[0], preferred_element_type=jnp.float32)
    up_part = jnp.dot(expert_rows, expert_up[0], preferred_element_type=jnp.float32)
    inner_act = (jax.nn.silu(gate_part) * up_part).astype(jnp.bfloat16)
    down_width = expert_down.shape[2]
    weight_rows = expert_down[0]
    expert_sum = jnp.dot(
        lax.all_gather(inner_act, "tp", axis=1, tiled=True),
        weight_rows,
        preferred_element_type=jnp.float32,
    )
    expert_out = expert_sum.astype(jnp.bfloat16).reshape(expert_count, capacity, down_width)
    returned = lax.all_to_all(expert_out, "sp", split_axis=0, concat_axis=0, tiled=True)
    per_route = returned.reshape(expert_count * capacity, down_width)[slot_index]
    weighted = per_route.astype(jnp.float32) * route_weight.reshape(-1)[:, None]
    token_sum = jnp.sum(weighted.reshape(tok_count, top_count, down_width), axis=1)
    moe_rows = lax.all_gather(token_sum.astype(jnp.bfloat16), "tp", axis=1, tiled=True).astype(
        token_sum.dtype
    )
    return (stream + moe_rows).astype(jnp.bfloat16)


def solution(mesh):
    in_specs = (
        P("sp", None),
        P("sp", "tp", None),
        P("sp", "tp", None),
        P("sp", "tp", None),
        P("tp"),
        P(),
        P("tp", None),
        P(),
        P("sp", None, "tp"),
        P("sp", None, "tp"),
        P("sp", None, "tp"),
        P("sp", None),
        P("sp", None),
    )
    out_specs = P("sp", None)
    return jax.shard_map(shards, mesh=mesh, in_specs=in_specs, out_specs=out_specs, check_vma=False)
```

profile of v0, /device:TPU:0, one launch (start us, length us, event | category | flops | bytes accessed | tf_op | source)
XLA Modules:
  0.0 432.6 jit_solution(9238692892261272300)
XLA Ops:
  6.5 1.8 copy.21
  8.5 1.7 copy.23
  10.2 0.8 copy.30
  13.2 1.1 reduce-window.6
  14.6 26.3 %all-gather.6.cloned.1.call-done = bf16[2048,4,128]{2,0,1:T(8,128)(2,1)} async-done(((bf16[256,4,128]{2,0,1:T(8,128)(2,1)}), bf16[2048,4,128]{2,0,1:T(8,128)(2,1)}) %all-gather.6.cloned.1.call-update) | async-done | bytes 2097168 | tf_op jit(solution)/shard_map/all_gather | solution.py:61
  40.9 4.1 copy.25
  45.0 26.1 %all-gather.8.cloned.1.call-done = bf16[2048,4,128]{2,0,1:T(8,128)(2,1)} async-done(((bf16[256,4,128]{2,0,1:T(8,128)(2,1)}), bf16[2048,4,128]{2,0,1:T(8,128)(2,1)}) %all-gather.8.cloned.1.call-update) | async-done | bytes 2097168 | tf_op jit(solution)/shard_map/all_gather | solution.py:62
  71.0 3.1 copy.26
  74.3 13.0 %while.21 = (s32[]{:T(128)}, f32[4,256]{1,0:T(4,128)S(1)}, f32[4,256]{1,0:T(4,128)S(1)}, f32[256,4,128]{2,0,1:T(8,128)S(1)}, f32[4,256]{1,0:T(4,128)S(1)}, /*ind...) while((s32[]{:T(128)}, f32[4,256]{1,0:T(4,128)S(1)}, ...), condition=%wide.region_7.8_spmd.clone, body=%wide.region_0.7_spmd.clone.sunk | while | flops 410655488 | bytes 26489292 | solution.py:97
  76.2 5.1 %conditional.3 = ((f32[4,256]{1,0:T(4,128)S(1)}, f32[4,256]{1,0:T(4,128)S(1)}, f32[256,4,128]{2,0,1:T(8,128)S(1)}, f32[4,256]{1,0:T(4,128)S(1)}, f32[4,256]{1,0:T(4,128)S(1)}, /*index=5*/f32[256,4,128]{2,0,1:T(8,128)S(1)})) conditional(s32[]{:T(128)} %convert_element_type.97, (f32[4,256]{1,0:T(4,128)S(1)}, f32[4,256]{1,0:T(4,128)S(1)}, ...), branch_computations={%region_1.1_spmd, %region_2.6_spmd} | conditional | flops 410655488 | bytes 26485864 | solution.py:95
  76.2 1.1 dynamic-slice_bitcast_fusion
  87.3 1.0 copy.27
  88.5 1.2 multiply_reduce_fusion.2
  89.9 1.7 convolution_convert_fusion
  91.9 0.8 dynamic-slice
  92.8 2.4 scatter_custom_fusion
  95.3 63.5 %all-reduce.2.cloned.1.call-done = bf16[256,2048]{1,0:T(8,128)(2,1)} async-done(((bf16[256,2048]{1,0:T(8,128)(2,1)}), bf16[256,2048]{1,0:T(8,128)(2,1)}) %all-reduce.2.cloned.1.call-update) | async-done | bytes 1048592 | tf_op jit(solution)/shard_map/psum | solution.py:111
  158.8 1.6 multiply_reduce_fusion
  160.6 4.0 gather_fusion
  164.8 31.1 %all_to_all.10 = bf16[8,128,512]{2,1,0:T(8,128)(2,1)} all-to-all(bf16[8,128,512]{2,1,0:T(8,128)(2,1)S(1)} %broadcast_select_fusion), channel_id=1, replica_groups=mesh['sp'=8,'tp'=4] {'sp'}, dimensions={0} | all-to-all | bytes 2097152 | tf_op jit(solution)/shard_map/all_to_all | solution.py:141
  196.1 50.3 %all-gather.10.cloned.1.call-done = bf16[8,128,2048]{2,1,0:T(8,128)(2,1)} async-done(((bf16[8,128,512]{2,1,0:T(8,128)(2,1)}), bf16[8,128,2048]{2,1,0:T(8,128)(2,1)}) %all-gather.10.cloned.1.call-update) | async-done | bytes 4194320 | tf_op jit(solution)/shard_map/all_gather | solution.py:142
  246.4 7.6 %fusion.24 = f32[1024,1024]{1,0:T(8,128)S(1)} fusion(bf16[1024,2048]{1,0:T(8,128)(2,1)} %bitcast.87, bf16[1,2048,1024]{2,1,0:T(8,128)(2,1)} %param.26), kind=kOutput, calls=%fused_computation.38 | convolution fusion | flops 4294967296 | bytes 12582912 | tf_op jit(solution)/shard_map/dot_general | solution.py:145
  254.1 6.4 %multiply_convert_fusion = bf16[1024,1024]{1,0:T(8,128)(2,1)} fusion(f32[1024,1024]{1,0:T(8,128)S(1)} %fusion.24, bf16[1024,2048]{1,0:T(8,128)(2,1)S(1)} %bitcast.88, bf16[1,2048,1024]{2,1,0:T(8,128)(2,1)S(1)} %copy-done.11), kind=kOutput, calls=%fused_computation.42 | convolution fusion | flops 4301258752 | bytes 14680064 | tf_op jit(solution)/shard_map/dot_general | solution.py:144
  260.5 87.6 %all-gather.12.cloned.1.call-done = bf16[1024,4096]{1,0:T(8,128)(2,1)} async-done(((bf16[1024,1024]{1,0:T(8,128)(2,1)}), bf16[1024,4096]{1,0:T(8,128)(2,1)}) %all-gather.12.cloned.1.call-update) | async-done | bytes 8388624 | tf_op jit(solution)/shard_map/all_gather | solution.py:150
  348.1 10.0 %fusion.30 = bf16[1024,512]{1,0:T(8,128)(2,1)} fusion(bf16[1024,4096]{1,0:T(8,128)(2,1)} %all-gather.12.cloned.1.call-done, bf16[1,4096,512]{2,1,0:T(8,128)(2,1)} %param.27), kind=kOutput, calls=%fused_computation.47 | convolution fusion | flops 4295491584 | bytes 13631488 | tf_op jit(solution)/shard_map/dot_general | solution.py:149
  358.2 4.7 %all-to-all-start.1 = ((bf16[8,128,512]{2,1,0:T(8,128)(2,1)}), bf16[8,128,512]{2,1,0:T(8,128)(2,1)S(1)}, u32[]{:S(2)}, u32[]{:S(2)}) async-start(bf16[8,128,512]{2,1,0:T(8,128)(2,1)} %bitcast.80), calls=%async_computation.1 | async-start | bytes 2097152 | tf_op jit(solution)/shard_map/all_to_all | solution.py:155
  363.1 26.4 %all-to-all-done.1 = bf16[8,128,512]{2,1,0:T(8,128)(2,1)S(1)} async-done(((bf16[8,128,512]{2,1,0:T(8,128)(2,1)}), bf16[8,128,512]{2,1,0:T(8,128)(2,1)S(1)}, u32[]{:S(2)}, u32[]{:S(2)}) %all-to-all-start.1) | async-done | bytes 1048608 | tf_op jit(solution)/shard_map/all_to_all | solution.py:155
  389.5 2.6 gather_fusion.1
  392.1 2.8 reshape.181
  394.8 3.3 multiply_reduce_fusion.1
  398.2 24.5 %all-gather.14.cloned.1.call-done = bf16[256,2048]{1,0:T(8,128)(2,1)} async-done(((bf16[256,512]{1,0:T(8,128)(2,1)}), bf16[256,2048]{1,0:T(8,128)(2,1)}) %all-gather.14.cloned.1.call-update) | async-done | bytes 1048592 | tf_op jit(solution)/shard_map/all_gather | solution.py:159
  422.7 3.1 add_convert_fusion
  (102 shorter events, 10.5 us)
Async XLA Ops:
  6.5 83.3 %copy-start = (bf16[512,2048]{1,0:T(8,128)(2,1)S(1)}, bf16[512,2048]{1,0:T(8,128)(2,1)}, u32[]{:S(2)}) copy-start(bf16[512,2048]{1,0:T(8,128)(2,1)} %param.23) | copy-start | bytes 6291460
  6.5 6.0 %copy-start.4 = (bf16[256,4,128]{2,1,0:T(4,128)(2,1)S(1)}, bf16[256,4,128]{2,1,0:T(4,128)(2,1)}, u32[]{:S(2)}) copy-start(bf16[256,4,128]{2,1,0:T(4,128)(2,1)} %param.18) | copy-start | bytes 786436
  6.5 34.3 %all-gather.6.cloned.1.call-start = ((), (), s32[]{:S(2)}) async-start(), calls=%async_computation.2 | async-start | bytes 2359296 | tf_op jit(solution)/shard_map/all_gather | solution.py:61
  8.4 62.6 %all-gather.8.cloned.1.call-start = ((), (), s32[]{:S(2)}) async-start(), calls=%async_computation.3 | async-start | bytes 2359296 | tf_op jit(solution)/shard_map/all_gather | solution.py:62
  10.2 148.6 %all-reduce.2.cloned.1.call-start = ((), (), s32[]{:S(2)}) async-start(), calls=%async_computation.4 | async-start | bytes 2097152 | tf_op jit(solution)/shard_map/psum | solution.py:111
  14.6 30.4 %copy-start.5 = (s32[8,5]{0,1:T(8,128)}, s32[8,5]{0,1:T(8,128)S(1)}, u32[]{:S(2)}) copy-start(s32[8,5]{0,1:T(8,128)S(1)} %reduce-window.9) | copy-start | bytes 484
  78.4 1.6 copy-start.1
  87.2 1.2 copy-start.9
  87.3 2.4 copy-start.10
  89.8 1.8 copy-start.6
  89.8 2.9 slice-start
  89.8 2.9 copy-start.7
  89.8 69.0 %copy-start.2 = (bf16[256,2048]{1,0:T(8,128)(2,1)S(1)}, bf16[256,2048]{1,0:T(8,128)(2,1)}, u32[]{:S(2)}) copy-start(bf16[256,2048]{1,0:T(8,128)(2,1)} %param.17) | copy-start | bytes 3145732
  91.6 154.9 %all-gather.10.cloned.1.call-start = ((), (), s32[]{:S(2)}) async-start(), calls=%async_computation.5 | async-start | bytes 5242880 | tf_op jit(solution)/shard_map/all_gather | solution.py:142
  195.9 152.2 %all-gather.12.cloned.1.call-start = ((), (), s32[]{:S(2)}) async-start(), calls=%async_computation.6 | async-start | bytes 10485760 | tf_op jit(solution)/shard_map/all_gather | solution.py:150
  246.4 7.7 %copy-start.11 = (bf16[1,2048,1024]{2,1,0:T(8,128)(2,1)S(1)}, bf16[1,2048,1024]{2,1,0:T(8,128)(2,1)}, u32[]{:S(2)}) copy-start(bf16[1,2048,1024]{2,1,0:T(8,128)(2,1)} %param.25) | copy-start | bytes 12582916
  246.4 7.7 %copy-start.12 = (bf16[8,128,2048]{2,1,0:T(8,128)(2,1)S(1)}, bf16[8,128,2048]{2,1,0:T(8,128)(2,1)}, u32[]{:S(2)}) copy-start(bf16[8,128,2048]{2,1,0:T(8,128)(2,1)} %all-gather.10.cloned.1.call-done) | copy-start | bytes 12582916
  358.2 4.8 %copy-start.8 = (f32[256,2]{0,1:T(2,128)S(1)}, f32[256,2]{0,1:T(2,128)}, u32[]{:S(2)}) copy-start(f32[256,2]{0,1:T(2,128)} %param.29) | copy-start | bytes 6148
  358.2 31.3 %all-to-all-start.1 = ((bf16[8,128,512]{2,1,0:T(8,128)(2,1)}), bf16[8,128,512]{2,1,0:T(8,128)(2,1)S(1)}, u32[]{:S(2)}, u32[]{:S(2)}) async-start(bf16[8,128,512]{2,1,0:T(8,128)(2,1)} %bitcast.80), calls=%async_computation.1 | async-start | bytes 2097152 | tf_op jit(solution)/shard_map/all_to_all | solution.py:155
  362.9 59.8 %all-gather.14.cloned.1.call-start = ((), (), s32[]{:S(2)}) async-start(), calls=%async_computation.7 | async-start | bytes 1310720 | tf_op jit(solution)/shard_map/all_gather | solution.py:159
  392.1 30.6 %copy-start.3 = (bf16[256,2048]{1,0:T(8,128)(2,1)S(1)}, bf16[256,2048]{1,0:T(8,128)(2,1)}, u32[]{:S(2)}) copy-start(bf16[256,2048]{1,0:T(8,128)(2,1)} %param.17) | copy-start | bytes 3145732
Sparse Core Ops, SparseCore 0:
  8.9 31.8 all-gather.5
  42.5 28.5 all-gather.7
  91.7 67.0 all-reduce.1
  196.0 50.3 all-gather.9
  260.6 87.4 all-gather.11
  398.3 24.3 all-gather.13
where the time goes:
time: 434 us; the launch traced here: 433 us
  waiting for transfers between devices  305 us (70%)
  local copies, waits for them, and re-layouts  32.3 us (7%)
  blocking collectives  31.1 us (7%)
  matrix products  28.1 us (6%)
  between operations  13.8 us (3%)
  other arithmetic  11.8 us (3%)
  loops' own time  5.62 us (1%)
  starting transfers between devices  5.12 us (1%)
    all_gather x1, waiting for transfers between devices, shards(): lax.all_gather(inner_act, 'tp', axis=1, tiled=True)  87.6 us
    psum x1, waiting for transfers between devices, shards(): lax.psum(partial_proj.astype(jnp.bfloat16), 'tp').astype(jnp.float32)  63.5 us
    all_gather x1, waiting for transfers between devices, shards(): arrived = lax.all_gather(landed, 'tp', axis=2, tiled=True)  50.3 us
    all_to_all x1, blocking collectives, shards(): lax.all_to_all(outgoing, 'sp', split_axis=0, concat_axis=0, tiled=True)  31.1 us
    all_to_all x1, waiting for transfers between devices, shards(): lax.all_to_all(expert_out, 'sp', split_axis=0, concat_axis=0, tiled=True)  26.4 us
    all_gather x1, waiting for transfers between devices, shards(): key_piece = lax.all_gather(key_vectors, 'sp', axis=0, tiled=True)  26.3 us
    all_gather x1, waiting for transfers between devices, shards(): value_piece = lax.all_gather(value_rows, 'sp', axis=0, tiled=True)  26.1 us
    all_gather x1, waiting for transfers between devices, shards(): lax.all_gather(token_sum.astype(jnp.bfloat16), 'tp', axis=1, tiled=True)  24.5 us
  transfers between devices with their start and end apart: 7, of which 7 were waited for; matrix products, arithmetic and copies ran while one was open for 3% of the time, Pallas kernels for 0%

commit v1 on v0

--- a/solution.py
+++ b/solution.py
@@ -1,8 +1,11 @@
+import functools
 import math
 
 import jax
 import jax.numpy as jnp
 from jax import lax
+from jax.experimental import pallas as pl
+from jax.experimental.pallas import tpu as pltpu
 from jax.sharding import PartitionSpec as P
 
 GROUPS = 4
@@ -162,6 +165,515 @@
     return (stream + moe_rows).astype(jnp.bfloat16)
 
 
+MESH = pl.DeviceIdType.MESH
+F32 = jnp.float32
+BF16 = jnp.bfloat16
+
+
+def remote(src, dst, send_sem, recv_sem, sp, tp):
+    return pltpu.make_async_remote_copy(
+        src_ref=src,
+        dst_ref=dst,
+        send_sem=send_sem,
+        recv_sem=recv_sem,
+        device_id={"sp": sp, "tp": tp},
+        device_id_type=MESH,
+    )
+
+
+def mixed_dot(left, right, contract):
+    return lax.dot_general(left, right, (contract, ((), ())), preferred_element_type=F32)
+
+
+def attention_kernel(
+    n, tps, heads, head_width,
+    q_ref, kv_ref, wt_ref, wd_ref, lam_ref, gain_ref, ow_ref, res_ref, fg_ref,
+    stream_ref, normed_ref, wdr_ref, wtall_ref,
+    kvall, qs, highs, totals, acc, att, part, rbuf, sq_send, sq_recv,
+    local_sem, kv_next, kv_sib, kv_recv, wd_send, wd_recv, wt_send, wt_recv,
+    rs_send, rs_recv, sq_ss, sq_rs,
+):
+    sp = lax.axis_index("sp")
+    tp = lax.axis_index("tp")
+    z, c = sp // 2, sp % 2
+    zs = n // 2
+    sib = 2 * z + 1 - c
+    toks = q_ref.shape[0]
+    width = heads * head_width
+    half = head_width // 2
+    own = pltpu.make_async_copy(kv_ref, kvall.at[sp], local_sem)
+    own.start()
+    wd_rows = wd_ref.shape[0] // tps
+
+    def wd_copy(d):
+        to = (tp + d) % tps
+        return remote(
+            wd_ref.at[pl.ds(pl.multiple_of(to * wd_rows, wd_rows), wd_rows), :],
+            wdr_ref.at[tp], wd_send.at[d], wd_recv.at[d], sp, to,
+        )
+
+    def wt_copy(d):
+        return remote(wt_ref, wtall_ref.at[sp], wt_send.at[d], wt_recv.at[d], (sp + d) % n, tp)
+
+    for d in range(1, n):
+        wt_copy(d).start()
+    for d in range(1, tps):
+        wd_copy(d).start()
+    wtall_ref[sp] = wt_ref[...]
+
+    lane = lax.broadcasted_iota(jnp.int32, (toks, head_width), 1)
+    scale = half ** (-0.5)
+    for h in range(heads):
+        block = q_ref[:, h * head_width : (h + 1) * head_width].astype(F32) * scale
+        qs[2 * h] = jnp.where(lane < half, block, 0.0).astype(BF16)
+        qs[2 * h + 1] = jnp.where(lane >= half, block, 0.0).astype(BF16)
+    highs[...] = jnp.full_like(highs, -1e30)
+    totals[...] = jnp.zeros_like(totals)
+    acc[...] = jnp.zeros_like(acc)
+    rows = lax.broadcasted_iota(jnp.int32, (toks, toks), 0)
+    cols = lax.broadcasted_iota(jnp.int32, (toks, toks), 1)
+
+    def process(b):
+        seen = cols + b * toks <= rows + sp * toks
+        for h in range(heads):
+            keys = kvall[b, :, h * head_width : (h + 1) * head_width]
+            vals = kvall[b, :, width + h * head_width : width + (h + 1) * head_width]
+            for u in (2 * h, 2 * h + 1):
+                scores = mixed_dot(qs[u], keys, ((1,), (1,)))
+                scores = jnp.where(seen, scores, -1e30)
+                old = highs[u]
+                high = jnp.maximum(old, jnp.max(scores, axis=1, keepdims=True))
+                shrink = jnp.exp(old - high)
+                weights = jnp.exp(scores - high)
+                totals[u] = shrink * totals[u] + jnp.sum(weights, axis=1, keepdims=True)
+                blended = mixed_dot(weights.astype(BF16), vals, ((1,), (0,)))
+                acc[u] = shrink * acc[u] + blended
+                highs[u] = high
+
+    def next_copy(b):
+        return remote(kvall.at[b], kvall.at[b], kv_next.at[b], kv_recv.at[b], sp + 2, tp)
+
+    def sib_copy(b):
+        return remote(kvall.at[b], kvall.at[b], kv_sib.at[b], kv_recv.at[b], sib, tp)
+
+    own.wait()
+
+    def visit(j, carry):
+        b = 2 * (z - j) + c
+        other = 2 * (z - j) + 1 - c
+
+        @pl.when(j > 0)
+        def _():
+            sib_copy(b).wait_recv()
+
+        @pl.when(z < zs - 1)
+        def _():
+            next_copy(b).start()
+
+        @pl.when(jnp.logical_or(j > 0, c == 0))
+        def _():
+            sib_copy(b).start()
+
+        process(b)
+
+        @pl.when(jnp.logical_or(j > 0, c == 1))
+        def _():
+            sib_copy(other).wait_recv()
+            process(other)
+
+        return carry
+
+    lax.fori_loop(0, z + 1, visit, 0)
+
+    for h in range(heads):
+        first = acc[2 * h] / totals[2 * h]
+        second = acc[2 * h + 1] / totals[2 * h + 1]
+        mix = first - lam_ref[h] * second
+        mix = mix * lax.rsqrt(jnp.mean(mix * mix, axis=1, keepdims=True) + norm_eps) * gain_ref[...]
+        att[:, h * head_width : (h + 1) * head_width] = mix.astype(BF16)
+    piece = ow_ref.shape[1] // tps
+
+    def projected(to):
+        return jnp.dot(
+            att[...], ow_ref[:, pl.ds(pl.multiple_of(to * piece, piece), piece)],
+            preferred_element_type=F32,
+        )
+
+    def rs_copy(d):
+        return remote(
+            part.at[d], rbuf.at[d], rs_send.at[d], rs_recv.at[d], sp, (tp + d) % tps
+        )
+
+    for d in range(1, tps):
+        part[d] = projected((tp + d) % tps).astype(BF16)
+        rs_copy(d).start()
+    mine = pl.ds(pl.multiple_of(tp * piece, piece), piece)
+    total = projected(tp)
+    for d in range(1, tps):
+        rs_copy(d).wait_recv()
+        total = total + rbuf[d].astype(F32)
+    stream = res_ref[:, mine].astype(F32) + total
+    stream_ref[...] = stream
+    eye = rows == cols
+    squares = jnp.sum(stream * stream, axis=1, keepdims=True)
+    as_row = jnp.sum(jnp.where(eye, squares, 0.0), axis=0, keepdims=True)
+    sq_send[...] = jnp.broadcast_to(as_row, sq_send.shape)
+
+    def sq_copy(d):
+        return remote(
+            sq_send, sq_recv.at[d], sq_ss.at[d], sq_rs.at[d], sp, (tp + d) % tps
+        )
+
+    for d in range(1, tps):
+        sq_copy(d).start()
+    for d in range(1, tps):
+        sq_copy(d).wait_recv()
+        as_row = as_row + sq_recv[d, 0:1, :]
+    as_col = jnp.sum(jnp.where(eye, as_row, 0.0), axis=1, keepdims=True)
+    mean = as_col * (1.0 / (piece * tps))
+    normed_ref[...] = (stream * lax.rsqrt(mean + norm_eps) * fg_ref[:, mine]).astype(BF16)
+
+    for d in range(1, tps):
+        sq_copy(d).wait_send()
+        rs_copy(d).wait_send()
+        wd_copy(d).wait()
+    for d in range(1, n):
+        wt_copy(d).wait()
+
+    def drain(j, carry):
+        b = 2 * (z - j) + c
+
+        @pl.when(z < zs - 1)
+        def _():
+            next_copy(b).wait_send()
+
+        @pl.when(jnp.logical_or(j > 0, c == 0))
+        def _():
+            sib_copy(b).wait_send()
+
+        return carry
+
+    lax.fori_loop(0, z + 1, drain, 0)
+
+
+def expert_kernel(
+    n, tps, cap,
+    normed_ref, stream_ref, sel_ref, selt_ref, wtall_ref, gate_ref, up_ref, wd_ref, wdr_ref,
+    out_ref,
+    xs, xall, wg, wu, wdv, hid, keep, away, near, rsend, rrecv, back, ret,
+    w_sem, x_send, x_tp, x_sib, x_recv, n_send, n_recv, r_send, r_recv, b_send, b_recv,
+    o_send, o_recv,
+):
+    sp = lax.axis_index("sp")
+    tp = lax.axis_index("tp")
+    z, c = sp // 2, sp % 2
+    zs = n // 2
+    sib = 2 * z + 1 - c
+    piece = normed_ref.shape[1]
+    wd_rows = wdv.shape[1]
+    loads = [
+        pltpu.make_async_copy(gate_ref.at[0], wg, w_sem.at[0]),
+        pltpu.make_async_copy(up_ref.at[0], wu, w_sem.at[1]),
+        pltpu.make_async_copy(
+            wd_ref.at[pl.ds(pl.multiple_of(tp * wd_rows, wd_rows), wd_rows), :],
+            wdv.at[tp], w_sem.at[2],
+        ),
+    ]
+    for d in range(1, tps):
+        peer = (tp + d) % tps
+        loads.append(pltpu.make_async_copy(wdr_ref.at[peer], wdv.at[peer], w_sem.at[2 + d]))
+    for load in loads:
+        load.start()
+
+    def spot(src, core, part):
+        return xall.at[
+            src,
+            pl.ds(pl.multiple_of(core * cap, cap), cap),
+            pl.ds(pl.multiple_of(part * piece, piece), piece),
+        ]
+
+    def x_copy(s):
+        group = (z + s) % zs
+        return remote(
+            xs.at[s], spot(z, c, tp), x_send.at[s], x_recv.at[z, c, tp], 2 * group + c, tp
+        )
+
+    def x_wait(src, core, part):
+        here = spot(src, core, part)
+        remote(here, here, x_send.at[0], x_recv.at[src, core, part], sib, tp).wait_recv()
+
+    def tp_copy(src, d):
+        here = spot(src, c, tp)
+        return remote(
+            here, here, x_tp.at[src, d], x_recv.at[src, c, tp], sp, (tp + d) % tps
+        )
+
+    def sib_copy(src, part):
+        here = spot(src, c, part)
+        return remote(here, here, x_sib.at[src, part], x_recv.at[src, c, part], sib, tp)
+
+    for s in list(range(1, zs)) + [0]:
+        group = (z + s) % zs
+        picked = jnp.dot(
+            sel_ref[pl.ds(pl.multiple_of(group * cap, cap), cap), :], normed_ref[...],
+            preferred_element_type=F32,
+        ).astype(BF16)
+        if s:
+            xs[s] = picked
+            x_copy(s).start()
+        else:
+            spot(z, c, tp)[...] = picked
+
+    def origin(s):
+        return (z - s + zs) % zs
+
+    def arrive(s):
+        src = origin(s)
+
+        @pl.when(s > 0)
+        def _():
+            x_wait(src, c, tp)
+
+        for d in range(1, tps):
+            tp_copy(src, d).start()
+        sib_copy(src, tp).start()
+
+    def complete(s):
+        src = origin(s)
+        for d in range(1, tps):
+            x_wait(src, c, (tp + d) % tps)
+            sib_copy(src, (tp + d) % tps).start()
+        for part in range(tps):
+            x_wait(src, 1 - c, part)
+
+    def near_copy(src):
+        return remote(away.at[src], near.at[src], n_send.at[src], n_recv.at[src], sib, tp)
+
+    tile = 256
+    eye = lax.broadcasted_iota(jnp.int32, (cap, cap), 0) == lax.broadcasted_iota(
+        jnp.int32, (cap, cap), 1
+    )
+    experts = wtall_ref.shape[1]
+    which = lax.broadcasted_iota(jnp.int32, (experts, cap), 0)
+
+    def weight_col(src, core):
+        table = wtall_ref[2 * src + core]
+        row = jnp.sum(jnp.where(which == sp, table, 0.0), axis=0, keepdims=True)
+        return jnp.sum(jnp.where(eye, row, 0.0), axis=1, keepdims=True)
+
+    def ffn(s):
+        src = origin(s)
+
+        def one(i, carry):
+            at = pl.ds(pl.multiple_of(i * tile, tile), tile)
+            x = xall[src]
+            gate = jnp.dot(x, wg[:, at], preferred_element_type=F32)
+            up = jnp.dot(x, wu[:, at], preferred_element_type=F32)
+            hid[:, at] = (gate / (1.0 + jnp.exp(-gate)) * up).astype(BF16)
+            return carry
+
+        lax.fori_loop(0, wg.shape[1] // tile, one, 0)
+        keep_w = weight_col(src, c)
+        away_w = weight_col(src, 1 - c)
+        keep_rows = pl.ds(pl.multiple_of(c * cap, cap), cap)
+        away_rows = pl.ds(pl.multiple_of((1 - c) * cap, cap), cap)
+
+        def two(j, carry):
+            away[src, j] = (
+                jnp.dot(hid[away_rows, :], wdv[j], preferred_element_type=F32) * away_w
+            ).astype(BF16)
+            keep[src, j] = jnp.dot(hid[keep_rows, :], wdv[j], preferred_element_type=F32) * keep_w
+            return carry
+
+        lax.fori_loop(0, tps, two, 0)
+        near_copy(src).start()
+
+    def r_copy(src, d):
+        return remote(
+            rsend.at[src, d], rrecv.at[src, d], r_send.at[src, d], r_recv.at[src, d],
+            sp, (tp + d) % tps,
+        )
+
+    def spread(s):
+        src = origin(s)
+        near_copy(src).wait_recv()
+        for d in range(1, tps):
+            to = (tp + d) % tps
+            rsend[src, d] = (keep[src, to] + near[src, to].astype(F32)).astype(BF16)
+            r_copy(src, d).start()
+
+    def b_copy(src):
+        return remote(
+            back.at[src], ret.at[z], b_send.at[src], b_recv.at[z], 2 * src + c, tp
+        )
+
+    def finish(s):
+        src = origin(s)
+        total = keep[src, tp] + near[src, tp].astype(F32)
+        for d in range(1, tps):
+            r_copy(src, d).wait_recv()
+            total = total + rrecv[src, d].astype(F32)
+
+        @pl.when(s == 0)
+        def _():
+            ret[z] = total.astype(BF16)
+
+        @pl.when(s > 0)
+        def _():
+            back[src] = total.astype(BF16)
+            b_copy(src).start()
+
+    arrive(0)
+    for load in loads:
+        load.wait()
+
+    def step(s, carry):
+        pl.when(s + 1 < zs)(lambda: arrive(s + 1))
+
+        @pl.when(s < zs)
+        def _():
+            complete(s)
+            ffn(s)
+
+        pl.when(jnp.logical_and(s >= 1, s <= zs))(lambda: spread(s - 1))
+        pl.when(s >= 2)(lambda: finish(s - 2))
+        return carry
+
+    lax.fori_loop(0, zs + 2, step, 0)
+
+    for s in range(1, zs):
+        group = (z + s) % zs
+        remote(
+            back.at[group], ret.at[group], b_send.at[group], b_recv.at[group], sib, tp
+        ).wait_recv()
+    rows = ret[...].reshape(zs * cap, piece)
+    layer = stream_ref[...] + jnp.dot(selt_ref[...], rows, preferred_element_type=F32)
+    mine = out_ref.at[:, pl.ds(pl.multiple_of(tp * piece, piece), piece)]
+    mine[...] = layer.astype(BF16)
+
+    def o_copy(d):
+        return remote(mine, mine, o_send.at[d], o_recv.at[d], sp, (tp + d) % tps)
+
+    for d in range(1, tps):
+        o_copy(d).start()
+    for s in range(1, zs):
+        x_copy(s).wait_send()
+        b_copy(origin(s)).wait_send()
+    for src in range(zs):
+        near_copy(src).wait_send()
+        sib_copy(src, tp).wait_send()
+        for d in range(1, tps):
+            tp_copy(src, d).wait_send()
+            sib_copy(src, (tp + d) % tps).wait_send()
+            r_copy(src, d).wait_send()
+    for d in range(1, tps):
+        o_copy(d).wait()
+
+
+def paired_shards(
+    residual, queries, key_vectors, value_rows, head_lambda, head_gain, out_weight, ffn_gain,
+    expert_gate, expert_up, expert_down, routing, route_weight,
+):
+    n = lax.axis_size("sp")
+    tps = lax.axis_size("tp")
+    toks, heads, head_width = queries.shape
+    width = heads * head_width
+    model = residual.shape[1]
+    piece = model // tps
+    experts = n
+    per_group = experts // GROUPS
+    cap = toks // per_group
+    group = routing[:, 0] // per_group
+    member = (group[:, None] == jnp.arange(GROUPS, dtype=jnp.int32)[None, :]).astype(jnp.int32)
+    position = jnp.sum((jnp.cumsum(member, axis=0) - member) * member, axis=1)
+    slot = group * cap + position
+    slots = jnp.arange(GROUPS * cap, dtype=jnp.int32)
+    sel = (slots[:, None] == slot[None, :]).astype(BF16)
+    selt = (slot[:, None] == slots[None, :]).astype(BF16)
+    by_expert = jnp.sum(
+        jnp.where(
+            routing[:, :, None] == jnp.arange(experts, dtype=jnp.int32), route_weight[:, :, None], 0.0
+        ),
+        axis=1,
+    )
+    table = jnp.einsum(
+        "gst,tgp->gps",
+        sel.astype(F32).reshape(GROUPS, cap, toks),
+        by_expert.reshape(toks, GROUPS, per_group),
+        precision=lax.Precision.HIGHEST,
+    ).reshape(experts, cap)
+    kv = jnp.concatenate(
+        [key_vectors.reshape(toks, width), value_rows.reshape(toks, width)], axis=1
+    )
+    down = expert_down[0]
+    wd_rows = down.shape[0] // tps
+    vmem = pl.BlockSpec(memory_space=pltpu.VMEM)
+    smem = pl.BlockSpec(memory_space=pltpu.SMEM)
+    hbm = pl.BlockSpec(memory_space=pl.ANY)
+    dma = pltpu.SemaphoreType.DMA
+    units = 2 * heads
+    stream, normed, wdr, wtall = pl.pallas_call(
+        functools.partial(attention_kernel, n, tps, heads, head_width),
+        out_shape=(
+            jax.ShapeDtypeStruct((toks, piece), F32),
+            jax.ShapeDtypeStruct((toks, piece), BF16),
+            jax.ShapeDtypeStruct((tps, wd_rows, piece), BF16),
+            jax.ShapeDtypeStruct((n, experts, cap), F32),
+        ),
+        in_specs=[vmem, hbm, vmem, hbm, smem, vmem, vmem, vmem, vmem],
+        out_specs=(vmem, vmem, hbm, vmem),
+        scratch_shapes=[
+            pltpu.VMEM((n, toks, 2 * width), BF16),
+            pltpu.VMEM((units, toks, head_width), BF16),
+            pltpu.VMEM((units, toks, 1), F32),
+            pltpu.VMEM((units, toks, 1), F32),
+            pltpu.VMEM((units, toks, head_width), F32),
+            pltpu.VMEM((toks, width), BF16),
+            pltpu.VMEM((tps, toks, piece), BF16),
+            pltpu.VMEM((tps, toks, piece), BF16),
+            pltpu.VMEM((8, toks), F32),
+            pltpu.VMEM((tps, 8, toks), F32),
+            dma,
+            dma((n,)), dma((n,)), dma((n,)),
+            dma((tps,)), dma((tps,)), dma((n,)), dma((n,)),
+            dma((tps,)), dma((tps,)), dma((tps,)), dma((tps,)),
+        ],
+        compiler_params=pltpu.CompilerParams(has_side_effects=True),
+        name="attend",
+    )(
+        queries.reshape(toks, width), kv, table, down, head_lambda, head_gain.reshape(1, -1),
+        out_weight, residual, ffn_gain.reshape(1, -1),
+    )
+    zs = n // 2
+    return pl.pallas_call(
+        functools.partial(expert_kernel, n, tps, cap),
+        out_shape=jax.ShapeDtypeStruct((toks, model), BF16),
+        in_specs=[vmem, vmem, vmem, vmem, vmem, hbm, hbm, hbm, hbm],
+        out_specs=vmem,
+        scratch_shapes=[
+            pltpu.VMEM((zs, cap, piece), BF16),
+            pltpu.VMEM((zs, 2 * cap, model), BF16),
+            pltpu.VMEM(expert_gate.shape[1:], BF16),
+            pltpu.VMEM(expert_up.shape[1:], BF16),
+            pltpu.VMEM((tps, wd_rows, piece), BF16),
+            pltpu.VMEM((2 * cap, expert_gate.shape[2]), BF16),
+            pltpu.VMEM((zs, tps, cap, piece), F32),
+            pltpu.VMEM((zs, tps, cap, piece), BF16),
+            pltpu.VMEM((zs, tps, cap, piece), BF16),
+            pltpu.VMEM((zs, tps, cap, piece), BF16),
+            pltpu.VMEM((zs, tps, cap, piece), BF16),
+            pltpu.VMEM((zs, cap, piece), BF16),
+            pltpu.VMEM((zs, cap, piece), BF16),
+            dma((2 + tps,)),
+            dma((zs,)), dma((zs, tps)), dma((zs, tps)), dma((zs, 2, tps)),
+            dma((zs,)), dma((zs,)), dma((zs, tps)), dma((zs, tps)),
+            dma((zs,)), dma((zs,)), dma((tps,)), dma((tps,)),
+        ],
+        compiler_params=pltpu.CompilerParams(has_side_effects=True),
+        name="experts",
+    )(normed, stream, sel, selt, wtall, expert_gate, expert_up, down, wdr)
+
+
 def solution(mesh):
     in_specs = (
         P("sp", None),
@@ -179,4 +691,5 @@
         P("sp", None),
     )
     out_specs = P("sp", None)
-    return jax.shard_map(shards, mesh=mesh, in_specs=in_specs, out_specs=out_specs, check_vma=False)
+    paired = mesh.shape["sp"] == 2 * GROUPS
+    return jax.shard_map(paired_shards if paired else shards, mesh=mesh, in_specs=in_specs, out_specs=out_specs, check_vma=False)

time: 434 us -> 171 us (0.39)
  waiting for transfers between devices: 305 us -> 0 us
  Pallas kernels: 0 us -> 159 us
  blocking collectives: 31.1 us -> 0 us
  matrix products: 28.1 us -> 0.99 us
  local copies, waits for them, and re-layouts: 32.3 us -> 5.36 us
  between operations: 13.8 us -> 0.04 us
  other arithmetic: 11.8 us -> 5.25 us
  loops' own time: 5.62 us -> 0 us
  starting transfers between devices: 5.12 us -> 0 us
    all_gather x5 -> x0, waiting for transfers between devices: 215 us -> none  [the longest x1 87.6 us: shards(): lax.all_gather(inner_act, 'tp', axis=1, tiled=True)]
    pallas_call x0 -> x2, Pallas kernels: none -> 159 us  [the longest x1 85.5 us: paired_shards(): pl.pallas_call(functools.partial(expert_kernel, n, tps, cap), out_shape=j...]
    psum x1 -> x0, waiting for transfers between devices: 63.5 us -> none  [shards(): lax.psum(partial_proj.astype(jnp.bfloat16), 'tp').astype(jnp.float32)]
    all_to_all x1 -> x0, blocking collectives: 31.1 us -> none  [shards(): lax.all_to_all(outgoing, 'sp', split_axis=0, concat_axis=0, tiled=True)]
    dot_general x8 -> x1, matrix products: 28.1 us -> 0.99 us  [paired_shards(): jnp.einsum('gst,tgp->gps', sel.astype(F32).reshape(GROUPS, cap, toks), by...]
    all_to_all x1 -> x0, waiting for transfers between devices: 26.4 us -> none  [shards(): lax.all_to_all(expert_out, 'sp', split_axis=0, concat_axis=0, tiled=True)]
    unnamed x32 -> x2, local copies, waits for them, and re-layouts: 12.1 us -> 3.98 us
    gather x2 -> x0, local copies, waits for them, and re-layouts: 6.58 us -> none  [the longest x1 3.97 us: shards(): jnp.take(own_columns, slot_table, axis=0, mode='fill', fill_value=0)]
  transfers between devices with their start and end apart: 7 -> 0, of which waited for: 7 -> 0; matrix products, arithmetic and copies ran while one was open for 3% -> 0% of each run, Pallas kernels for 0% -> 0%
where the time goes in v1:
time: 171 us
  Pallas kernels  159 us (93%)
  local copies, waits for them, and re-layouts  5.36 us (3%)
  other arithmetic  5.25 us (3%)
    pallas_call x1, Pallas kernels, paired_shards(): pl.pallas_call(functools.partial(expert_kernel, n, tps, cap), out_shape=j...  85.5 us
    pallas_call x1, Pallas kernels, paired_shards(): pl.pallas_call(functools.partial(attention_kernel, n, tps, heads, head_wi...  73.5 us
    unnamed x2, local copies, waits for them, and re-layouts  3.98 us

profile of v1, /device:TPU:0, one launch (start us, length us, event | category | flops | bytes accessed | tf_op | source)
XLA Modules:
  0.0 170.6 jit_solution(17530489487954469515)
XLA Ops:
  0.0 0.7 fusion.9
  0.7 1.2 reduce-window.6
  1.9 0.1 slice.12
  2.0 0.1 copy.18
  2.2 0.1 copy.19
  2.2 0.1 add_bitcast_fusion
  2.4 0.7 select_reduce_fusion
  3.1 1.0 fusion.2
  4.1 0.8 fusion.sel_ref
  4.9 0.8 fusion.1.selt_ref
  5.7 1.7 copy.28
  7.4 1.1 copy_bitcast_fusion
  8.4 0.9 pad_maximum_fusion.kv_ref
  9.3 73.5 %attend.1 = (f32[256,512]{1,0:T(8,128)}, bf16[256,512]{1,0:T(8,128)(2,1)}, bf16[4,1024,512]{2,1,0:T(8,128)(2,1)}, f32[8,8,128]{2,1,0:T(8,128)}) custom-call(bf16[256,512]{1,0:T(8,128)(2,1)} %bitcast.43, bf16[256,1024]{1,0:T(8,128)(2,1)} %pad_maximum_fusion.kv_ref, f32[8,128]{1,0:T(8,128)} %bitcast.51, bf16[4096,512]{1,0:T(8,128)(2,1)} %bitcast.41, ...), custom_call_target="tpu_custom_call" | custom-call | tf_op jit(solution)/shard_map/attend/pallas_call | solution.py:615
  82.8 85.5 %experts.1 = bf16[256,2048]{1,0:T(8,128)(2,1)} custom-call(bf16[256,512]{1,0:T(8,128)(2,1)} %get-tuple-element.9.normed_ref, f32[256,512]{1,0:T(8,128)} %get-tuple-element.10.stream_ref, bf16[512,256]{1,0:T(8,128)(2,1)} %fusion.sel_ref, bf16[256,512]{1,0:T(8,128)(2,1)} %fusion.1.selt_ref, f32[8,8,128]{2,1,0:T(8,128)} %get-tuple-element.11.wtall_ref, ...), custom_call_target="tpu_custom_call" | custom-call | tf_op jit(solution)/shard_map/experts/pallas_call | solution.py:648
  168.3 2.3 %copy.30 = bf16[256,2048]{1,0:T(8,128)(2,1)} copy(bf16[256,2048]{1,0:T(8,128)(2,1)} %experts.1) | data formatting | bytes 2097152
  (8 shorter events, 0.1 us)
